TPU v7x, 256 devices: a 4x2x16 block of a 4x16x16 slice. The times are simulated.
256 devices in a mesh: grp: 2 (over y), sp: 32 (over z, core), tp: 4 (over x).
Axes of the slice: x: 4, y: 2, z: 16, core: 2. Of those that a mesh axis runs over, the one named last changes fastest.
The devices are a block of a 4x16x16 slice.
Arguments:
- resid_in: bfloat16 [16384, 2048], P(('grp', 'sp', 'tp')), parts along dimension 0, may hold values from -6 to 6
- query_narrow: bfloat16 [16384, 8, 128], P(('grp', 'sp'), 'tp'), parts along dimension 0, may hold values from -512 to 512
- key_narrow: bfloat16 [16384, 4, 128], P(('grp', 'sp'), 'tp'), parts along dimension 0, may hold values from -512 to 512
- value_narrow: bfloat16 [16384, 4, 128], P(('grp', 'sp'), 'tp'), parts along dimension 0, may hold values from -6 to 6
- query_wide: bfloat16 [16384, 8, 256], P(('grp', 'sp'), 'tp'), parts along dimension 0, may hold values from -512 to 512
- key_wide: bfloat16 [16384, 4, 256], P(('grp', 'sp'), 'tp'), parts along dimension 0, may hold values from -512 to 512
- value_wide: bfloat16 [16384, 4, 128], P(('grp', 'sp'), 'tp'), parts along dimension 0, may hold values from -6 to 6
- lambda_narrow: float32 [8], P('tp'), may hold values from 0.3 to 0.8
- lambda_wide: float32 [8], P('tp'), may hold values from 0.3 to 0.8
- head_gain: float32 [128], replicated, may hold values from 0.1 to 1.9
- out_narrow: bfloat16 [1024, 2048], P('tp'), may hold values from -0.125 to 0.125
- out_wide: bfloat16 [1024, 2048], P('tp'), may hold values from -0.125 to 0.125
- norm_gain: bfloat16 [2048], replicated, may hold values from 0.099609375 to 1.8984375
- up_weight: bfloat16 [2048, 8192], P('sp', 'tp'), may hold values from -0.125 to 0.125
- down_weight: bfloat16 [8192, 2048], P('tp', 'sp'), may hold values from -0.0625 to 0.0625
Outputs:
- mixed_out: bfloat16 [16384, 2048], P(('grp', 'sp', 'tp')), parts along dimension 0
There are 2 independent parts, one for each index of `grp`. A program takes and returns all parts, laid end to end along the dimension named above; an argument that names none is the same for every part. Nothing has to cross between parts.
All inputs are finite; a program needn't handle non-finite values.
Results may differ from a plain program's by a relative error of at most 0.018.
Values may be sent and summed in bfloat16 or wider, within the bound.
A program may use at most 128 MiB of HBM per device.

v0:
```python
import math

import jax
import jax.numpy as jnp
from jax import lax
from jax.sharding import PartitionSpec as P

NORM_EPS = 1e-06
OUT_SCALE = 0.8


def sent_together(arrays, axis, dim, along):
    ends, at = ([], 0)
    for a in arrays[:-1]:
        at += a.shape[along]
        ends.append(at)
    both = jnp.concatenate(arrays, axis=along)
    return tuple(jnp.split(lax.all_gather(both, axis, axis=dim, tiled=True), ends, axis=along))


def split_up(array, dim, peers):
    before, after = (array.shape[:dim], array.shape[dim + 1 :])
    return jnp.moveaxis(array.reshape(*before, peers, -1, *after), dim, 0)


def sent_and_summed(array, axis, dim):
    peers = lax.axis_size(axis)
    parts = lax.all_to_all(split_up(array, dim, peers), axis, 0, 0, tiled=True)
    return jnp.sum(parts.astype(jnp.float32), axis=0)


def laid_out(parts, dim):
    parts = jnp.moveaxis(parts, 0, dim)
    lengths = parts.shape
    return parts.reshape(*lengths[:dim], lengths[dim] * lengths[dim + 1], *lengths[dim + 2 :])


def copy_for_each(array, axis):
    copies = jnp.broadcast_to(array, (lax.axis_size(axis), *array.shape))
    return lax.all_to_all(copies, axis, split_axis=0, concat_axis=0, tiled=True)


def collect(array, axis, dim):
    return laid_out(copy_for_each(array, axis), dim)


def empty_state(query, key_head_stack, value_width):
    row_count, head_count = (query.shape[0], query.shape[1])
    group_size = head_count // key_head_stack
    row_top = jnp.full((key_head_stack, group_size, 2, row_count), -jnp.inf, jnp.float32)
    row_total = jnp.zeros((key_head_stack, group_size, 2, row_count), jnp.float32)
    weighted_values = jnp.zeros(
        (key_head_stack, group_size, 2, row_count, value_width), jnp.float32
    )
    return (row_top, row_total, weighted_values)


def absorb(states, query, key_rows, values):
    row_count, head_count = (query.shape[0], query.shape[1])
    key_head_stack = key_rows.shape[1]
    half_width = key_rows.shape[2] // 2
    group_size = head_count // key_head_stack
    value_width = values.shape[2]
    amount = key_rows.shape[0]
    block_rows = math.gcd(amount, 512)
    rotation_count = amount // block_rows
    grouped = query.reshape(row_count, key_head_stack, group_size, 2, half_width)
    key_block_list = key_rows.reshape(rotation_count, block_rows, key_head_stack, 2, half_width)
    value_blocks = values.reshape(rotation_count, block_rows, key_head_stack, value_width)

    def visit(running, kv_pair):
        row_top, row_total, weighted_values = running
        key_blk, value_blk = kv_pair
        scores = jnp.einsum(
            "tkgcd,skcd->kgcts", grouped, key_blk, preferred_element_type=jnp.float32
        ) * half_width ** (-0.5)
        new_top = jnp.maximum(row_top, jnp.max(scores, axis=-1))
        rescale = jnp.exp(row_top - new_top)
        powers = jnp.exp(scores - new_top[..., None])
        row_total = row_total * rescale + jnp.sum(powers, axis=-1)
        weighted_values = weighted_values * rescale[..., None] + jnp.einsum(
            "iodph,hie->iodpe",
            powers.astype(jnp.bfloat16),
            value_blk,
            preferred_element_type=jnp.float32,
        )
        return ((new_top, row_total, weighted_values), None)

    outcome, _ = lax.scan(visit, states, (key_block_list, value_blocks))
    return outcome


def finish(states, lambdas, gain_vec):
    row_top, row_total, weighted_values = states
    key_head_stack, group_size, row_count = (row_top.shape[0], row_top.shape[1], row_top.shape[3])
    value_width = weighted_values.shape[4]
    first_map = weighted_values[:, :, 0] / row_total[:, :, 0, :, None]
    second_map = weighted_values[:, :, 1] / row_total[:, :, 1, :, None]
    mixed = first_map - lambdas.reshape(key_head_stack, group_size)[:, :, None, None] * second_map
    normed = (
        mixed
        * lax.rsqrt(jnp.mean(mixed * mixed, axis=-1, keepdims=True) + NORM_EPS)
        * gain_vec
        * OUT_SCALE
    )
    normed = normed.astype(jnp.bfloat16).transpose(2, 0, 1, 3)
    return normed.reshape(row_count, key_head_stack * group_size * value_width)


def attend(
    query_narrow,
    key_narrow,
    value_narrow,
    query_wide,
    key_wide,
    value_wide,
    lambda_narrow,
    lambda_wide,
    head_gain,
):
    initial = (
        empty_state(query_narrow, key_narrow.shape[1], value_narrow.shape[2]),
        empty_state(query_wide, key_wide.shape[1], value_wide.shape[2]),
    )
    narrow_keys, narrow_values, wide_keys, wide_values = sent_together(
        (key_narrow, value_narrow, key_wide, value_wide), "sp", 0, 2
    )
    narrow_state = absorb(initial[0], query_narrow, narrow_keys, narrow_values)
    wide_state = absorb(initial[1], query_wide, wide_keys, wide_values)
    return (
        finish(narrow_state, lambda_narrow, head_gain),
        finish(wide_state, lambda_wide, head_gain),
    )


def shards(
    resid_in,
    query_narrow,
    key_narrow,
    value_narrow,
    query_wide,
    key_wide,
    value_wide,
    lambda_narrow,
    lambda_wide,
    head_gain,
    out_narrow,
    out_wide,
    norm_gain,
    up_weight,
    down_weight,
):
    att_narrow, att_wide = attend(
        query_narrow,
        key_narrow,
        value_narrow,
        query_wide,
        key_wide,
        value_wide,
        lambda_narrow,
        lambda_wide,
        head_gain,
    )
    projected = sent_and_summed(
        (
            jnp.dot(att_narrow, out_narrow, preferred_element_type=jnp.float32)
            + jnp.dot(att_wide, out_wide, preferred_element_type=jnp.float32)
        ).astype(jnp.bfloat16),
        "tp",
        0,
    )
    middle = (resid_in.astype(jnp.float32) + projected).astype(jnp.bfloat16)
    middle_f32 = middle.astype(jnp.float32)
    normed = middle_f32 * lax.rsqrt(
        jnp.mean(middle_f32 * middle_f32, axis=-1, keepdims=True) + NORM_EPS
    )
    normed = (normed * norm_gain.astype(jnp.float32)).astype(jnp.bfloat16)
    whole_rows = collect(normed, "tp", 0)
    up_collected = lax.all_gather(up_weight, "sp", axis=0, tiled=True)
    lifted = jnp.dot(whole_rows, up_collected, preferred_element_type=jnp.float32)
    activated = jnp.square(jax.nn.relu(lifted)).astype(jnp.bfloat16)
    partials = jnp.dot(
        activated,
        lax.all_gather(down_weight, "sp", axis=1, tiled=True),
        preferred_element_type=jnp.float32,
    )
    mixer_out = sent_and_summed(partials.astype(jnp.bfloat16), "tp", 0)
    return (middle_f32 + mixer_out).astype(jnp.bfloat16)


def solution(mesh):
    placed = (
        P(("grp", "sp", "tp"), None),
        P(("grp", "sp"), "tp", None),
        P(("grp", "sp"), "tp", None),
        P(("grp", "sp"), "tp", None),
        P(("grp", "sp"), "tp", None),
        P(("grp", "sp"), "tp", None),
        P(("grp", "sp"), "tp", None),
        P("tp"),
        P("tp"),
        P(),
        P("tp", None),
        P("tp", None),
        P(),
        P("sp", "tp"),
        P("tp", "sp"),
    )
    return jax.shard_map(
        shards, mesh=mesh, in_specs=placed, out_specs=P(("grp", "sp", "tp"), None), check_vma=False
    )
```

profile of v0, /device:TPU:40, one launch (start us, length us, event | category | flops | bytes accessed | tf_op | source)
XLA Modules:
  0.0 384.9 jit_solution(5291192769765145764)
XLA Ops:
  6.6 1.8 pad_maximum_fusion
  11.5 90.5 %all-gather.4.cloned.1.call-done = bf16[8192,1,640]{2,0,1:T(8,128)(2,1)} async-done(((bf16[256,1,640]{2,0,1:T(8,128)(2,1)}), bf16[8192,1,640]{2,0,1:T(8,128)(2,1)}) %all-gather.4.cloned.1.call-update) | async-done | bytes 10485776 | tf_op jit(solution)/shard_map/all_gather | solution.py:18
  102.0 5.2 %fusion.45 = (bf16[8192,1,128]{2,0,1:T(8,128)(2,1)}, bf16[8192,1,128]{2,0,1:T(8,128)(2,1)}, bf16[8192,1,128]{2,0,1:T(8,128)(2,1)S(1)}) fusion(bf16[8192,1,640]{2,0,1:T(8,128)(2,1)} %all-gather.4.cloned.1.call-done), kind=kLoop, calls=%fused_computation.88 | loop fusion | bytes 12582912 | tf_op jit(solution)/shard_map/split | solution.py:18
  107.3 3.2 reshape.284
  110.5 10.6 %copy.29 = bf16[16,512,1,2,64]{1,4,3,2,0:T(8,128)(2,1)} copy(bf16[16,512,1,2,64]{4,3,1,0,2:T(2,128)(2,1)} %reshape.284) | data formatting | bytes 4194304
  121.1 89.1 %while.30 = (s32[]{:T(128)}, f32[1,2,2,256]{3,1,2,0:T(2,128)S(1)}, f32[1,2,2,256]{3,1,2,0:T(2,128)}, f32[1,2,2,256,128]{4,3,2,1,0:T(8,128)}, bf16[16,512,1,2,64]...) while((s32[]{:T(128)}, f32[1,2,2,256]{3,1,2,0:T(2,128)S(1)}, ...), condition=%wide.region_3.4_spmd.clone, body=%wide.region_0.3_spmd.clone.sunk | while | flops 204871680 | bytes 12031193 | solution.py:89
  129.1 1.6 fusion.68
  145.8 1.6 fusion.68
  151.4 1.6 fusion.68
  157.0 1.6 fusion.68
  162.5 1.6 fusion.68
  168.1 1.6 fusion.68
  173.7 1.6 fusion.68
  179.2 1.6 fusion.68
  184.8 1.6 fusion.68
  190.3 1.6 fusion.68
  195.9 1.6 fusion.68
  201.4 1.7 fusion.68
  207.1 1.6 fusion.68
  210.2 2.0 copy.31
  212.2 4.6 %split.18 = bf16[8192,1,256]{2,0,1:T(8,128)(2,1)} slice(bf16[8192,1,640]{2,0,1:T(8,128)(2,1)} %all-gather.4.cloned.1.call-done), slice={[0:8192], [0:1], [256:512]} | slice | bytes 8388608 | tf_op jit(solution)/shard_map/split | solution.py:18
  216.8 7.0 %reshape.285 = bf16[16,512,1,2,128]{4,3,1,0,2:T(2,128)(2,1)} reshape(bf16[8192,1,256]{2,0,1:T(8,128)(2,1)} %split.18) | data formatting | bytes 8388608 | tf_op jit(solution)/shard_map/reshape | solution.py:68
  223.8 82.0 %while.31 = (s32[]{:T(128)}, f32[1,2,2,256]{3,1,2,0:T(2,128)S(1)}, f32[1,2,2,256]{3,1,2,0:T(2,128)S(1)}, f32[1,2,2,256,128]{4,3,2,1,0:T(8,128)}, bf16[16,512,1,2...) while((s32[]{:T(128)}, f32[1,2,2,256]{3,1,2,0:T(2,128)S(1)}, ...), condition=%wide.region_8.9_spmd.clone, body=%wide.region_5.0_spmd.clone.sunk | while | flops 271980544 | bytes 12784293 | solution.py:89
  231.6 1.6 fusion.73
  241.9 1.6 fusion.73
  247.0 1.6 fusion.73
  311.0 4.5 %all-to-all-start = ((bf16[4,64,2048]{2,1,0:T(8,128)(2,1)}), bf16[4,64,2048]{2,1,0:T(8,128)(2,1)S(1)}, u32[]{:S(2)}, u32[]{:S(2)}) async-start(bf16[4,64,2048]{2,1,0:T(8,128)(2,1)} %bitcast.16), calls=%async_computation | async-start | bytes 2097152 | tf_op jit(solution)/shard_map/all_to_all | solution.py:28
  315.4 15.6 %all-to-all-done = bf16[4,64,2048]{2,1,0:T(8,128)(2,1)S(1)} async-done(((bf16[4,64,2048]{2,1,0:T(8,128)(2,1)}), bf16[4,64,2048]{2,1,0:T(8,128)(2,1)S(1)}, u32[]{:S(2)}, u32[]{:S(2)}) %all-to-all-start) | async-done | bytes 1048608 | tf_op jit(solution)/shard_map/all_to_all | solution.py:28
  332.6 3.8 all-to-all-start.1
  336.5 14.4 %all-to-all-done.1 = bf16[4,64,2048]{2,1,0:T(8,128)(2,1)S(1)} async-done(((bf16[4,64,2048]{2,1,0:T(8,128)(2,1)}), bf16[4,64,2048]{2,1,0:T(8,128)(2,1)S(1)}, u32[]{:S(2)}, u32[]{:S(2)}) %all-to-all-start.1) | async-done | bytes 1048608 | tf_op jit(solution)/shard_map/all_to_all | solution.py:40
  350.9 10.3 %convolution_convert_fusion = bf16[256,2048]{1,0:T(8,128)(2,1)S(1)} fusion(bf16[2048,2048]{0,1:T(8,128)(2,1)} %all-gather.8.cloned.1.call-done, bf16[256,2048]{1,0:T(8,128)(2,1)S(1)} %bitcast.204, bf16[2048,2048]{1,0:T(8,128)(2,1)} %all-gather.6.cloned.1.call-done), kind=kOutput, calls=%fused_computation.52 | convolution fusion | flops 4297064448 | bytes 18874368 | tf_op jit(solution)/shard_map/dot_general | solution.py:182
  361.2 16.3 %all_to_all.15 = bf16[4,64,2048]{2,1,0:T(8,128)(2,1)S(1)} all-to-all(bf16[4,64,2048]{2,1,0:T(8,128)(2,1)S(1)} %bitcast.205), channel_id=1, replica_groups=mesh['grp'=2,'sp'=32,'tp'=4] {'tp'}, dimensions={0} | all-to-all | bytes 2097152 | tf_op jit(solution)/shard_map/all_to_all | solution.py:28
  (469 shorter events, 153.0 us)
Async XLA Ops:
  6.5 301.9 %copy-start = (bf16[256,2048]{1,0:T(8,128)(2,1)S(1)}, bf16[256,2048]{1,0:T(8,128)(2,1)}, u32[]{:S(2)}) copy-start(bf16[256,2048]{1,0:T(8,128)(2,1)} %param.29) | copy-start | bytes 3145732
  6.6 4.6 %copy-start.6 = (bf16[256,2,256]{2,1,0:T(2,128)(2,1)S(1)}, bf16[256,2,256]{2,1,0:T(2,128)(2,1)}, u32[]{:S(2)}) copy-start(bf16[256,2,256]{2,1,0:T(2,128)(2,1)} %param.23) | copy-start | bytes 786436
  6.6 95.5 %all-gather.4.cloned.1.call-start = ((), (), s32[]{:S(2)}) async-start(), calls=%async_computation.3 | async-start | bytes 10813440 | tf_op jit(solution)/shard_map/all_gather | solution.py:18
  8.5 328.0 %all-gather.6.cloned.1.call-start = ((), (), s32[]{:S(2)}) async-start(), calls=%async_computation.4 | async-start | bytes 8650752 | tf_op jit(solution)/shard_map/all_gather | solution.py:179
  9.3 327.2 %all-gather.8.cloned.1.call-start = ((), (), s32[]{:S(2)}) async-start(), calls=%async_computation.5 | async-start | bytes 8650752 | tf_op jit(solution)/shard_map/all_gather | solution.py:184
  122.5 3.5 copy-start.8
  128.1 3.5 copy-start.8
  133.7 3.5 copy-start.8
  139.2 1.1 copy-start.4
  139.2 3.5 copy-start.8
  144.8 3.5 copy-start.8
  150.4 3.5 copy-start.8
  155.9 3.5 copy-start.8
  161.5 3.5 copy-start.8
  167.1 3.5 copy-start.8
  172.6 3.5 copy-start.8
  178.2 3.5 copy-start.8
  183.8 3.5 copy-start.8
  189.3 3.5 copy-start.8
  194.9 3.5 copy-start.8
  200.4 3.5 copy-start.8
  206.0 3.5 copy-start.8
  223.8 83.3 %copy-start.10 = (f32[1,2,2,256]{3,1,2,0:T(2,128)S(1)}, f32[1,2,2,256]{3,1,2,0:T(2,128)}, u32[]{:S(2)}) copy-start(f32[1,2,2,256]{3,1,2,0:T(2,128)} %get-tuple-element.82) | copy-start | bytes 12292
  223.8 83.3 %copy-start.12 = (f32[2]{0:T(128)S(1)}, f32[2]{0:T(128)}, u32[]{:S(2)}) copy-start(f32[2]{0:T(128)} %param.27) | copy-start | bytes 28
  223.8 83.3 %copy-start.13 = (f32[2]{0:T(128)S(1)}, f32[2]{0:T(128)}, u32[]{:S(2)}) copy-start(f32[2]{0:T(128)} %param.26) | copy-start | bytes 28
  230.5 1.1 copy-start.2
  305.8 2.6 copy-start.14
  308.3 1.2 copy-start.1
  311.0 4.5 %copy-start.11 = (bf16[2048]{0:T(1024)(128)(2,1)S(1)}, bf16[2048]{0:T(1024)(128)(2,1)}, u32[]{:S(2)}) copy-start(bf16[2048]{0:T(1024)(128)(2,1)} %param.31) | copy-start | bytes 12292
  311.0 20.2 %copy-start.7 = (bf16[64,2048]{1,0:T(8,128)(2,1)S(1)}, bf16[64,2048]{1,0:T(8,128)(2,1)}, u32[]{:S(2)}) copy-start(bf16[64,2048]{1,0:T(8,128)(2,1)} %param.19) | copy-start | bytes 786436
  311.0 20.0 %all-to-all-start = ((bf16[4,64,2048]{2,1,0:T(8,128)(2,1)}), bf16[4,64,2048]{2,1,0:T(8,128)(2,1)S(1)}, u32[]{:S(2)}, u32[]{:S(2)}) async-start(bf16[4,64,2048]{2,1,0:T(8,128)(2,1)} %bitcast.16), calls=%async_computation | async-start | bytes 2097152 | tf_op jit(solution)/shard_map/all_to_all | solution.py:28
  332.6 18.2 %all-to-all-start.1 = ((bf16[4,64,2048]{2,1,0:T(8,128)(2,1)}), bf16[4,64,2048]{2,1,0:T(8,128)(2,1)S(1)}, u32[]{:S(2)}, u32[]{:S(2)}) async-start(bf16[4,64,2048]{2,1,0:T(8,128)(2,1)} %broadcast_in_dim.4), calls=%async_computation.1 | async-start | bytes 2097152 | tf_op jit(solution)/shard_map/all_to_all | solution.py:40
  (78 other events, 66.9 us)
Sparse Core Ops, SparseCore 0:
  9.2 92.7 all-gather.3
  103.9 73.4 all-gather.5
  179.3 73.6 all-gather.7
where the time goes:
time: 388 us; the launch traced here: 385 us
  waiting for transfers between devices  122 us (31%)
  local copies, waits for them, and re-layouts  109 us (28%)
  matrix products  94.4 us (24%)
  other arithmetic  18.6 us (5%)
  blocking collectives  16.3 us (4%)
  between operations  13.4 us (3%)
  starting transfers between devices  8.37 us (2%)
    all_gather x1, waiting for transfers between devices, sent_together(): lax.all_gather(both, axis, axis=dim, tiled=True)  90.5 us
    while x224, local copies, waits for them, and re-layouts  54.1 us
    dot_general x32, matrix products, visit(): jnp.einsum('iodph,hie->iodpe', powers.astype(jnp.bfloat16), value_blk, pr...  52.6 us
    dot_general x32, matrix products, visit(): jnp.einsum('tkgcd,skcd->kgcts', grouped, key_blk, preferred_element_type=...  29.6 us
    dynamic_slice x16, local copies, waits for them, and re-layouts, absorb(): outcome, _ = lax.scan(visit, states, (key_block_list, value_blocks))  18.2 us
    all_to_all x1, blocking collectives, sent_and_summed(): parts = lax.all_to_all(split_up(array, dim, peers), axis, 0, 0, tiled=True)  16.3 us
    all_to_all x1, waiting for transfers between devices, sent_and_summed(): parts = lax.all_to_all(split_up(array, dim, peers), axis, 0, 0, tiled=True)  15.6 us
    all_to_all x1, waiting for transfers between devices, copy_for_each(): return lax.all_to_all(copies, axis, split_axis=0, concat_axis=0, tiled=True)  14.4 us
  transfers between devices with their start and end apart: 5, of which 3 were waited for; matrix products, arithmetic and copies ran while one was open for 40% of the time, Pallas kernels for 0%

commit v1 on v0

v1 whole, which is shorter than its diff:
```python
import functools
import math

import jax
import jax.numpy as jnp
from jax import lax
from jax.experimental import pallas as pl
from jax.experimental.pallas import tpu as pltpu
from jax.sharding import PartitionSpec as P

NORM_EPS = 1e-06
OUT_SCALE = 0.8
LOG2E = math.log2(math.e)
MESH = pl.DeviceIdType.MESH
BF16 = jnp.bfloat16
F32 = jnp.float32

KV_N, KV_W, UP, DN_A, DN_B = range(5)
LAST_WAY = (1, 0, 1, 0, 1)
C_KV_N, C_KV_W, C_UP, C_DN = range(4)
CORE_LAST = (1, 0, 1, 1)
Y_UP, Y_DN = range(2)
KEY_PART = (0, 0, 2, 3)
VALUE_PART = (1, 1, 4, 4)
Q_TILE = 128
COLS = 512


def layer_kernel(
    nz, ntp, widths,
    q_ref, kn_ref, vn_ref, kw_ref, vw_ref, up_ref, dn_ref, on_ref, ow_ref, res_ref,
    lam_n_ref, lam_w_ref, head_gain_ref, norm_gain_ref,
    out_ref,
    kv, up, dn, outs, resid, acc, top, att, mid, nrm, act, part, mix, sumsq,
    zs, zr, cs, cr, ys, yr, xs, xr, os_, or_, rs, rr, as_, ar, ms, mr, ls,
):
    g, s, j = lax.axis_index("grp"), lax.axis_index("sp"), lax.axis_index("tp")
    z, c = s // 2, s % 2
    par = g % 2
    half = nz // 2
    rows = kv.shape[2]
    wrows = up.shape[1]
    hrows = wrows // 2
    qrows = wrows // 4
    own_rows = resid.shape[1]

    def sp_of(chip):
        return {"sp": 2 * lax.rem(chip + nz, nz) + c}

    z_to = (sp_of(z + 1), sp_of(z - 1))
    core_to = {"sp": 2 * z + 1 - c}
    y_to = {"grp": g + 1 - 2 * par}

    def tp_at(delta):
        return lax.rem(j + delta + ntp, ntp)

    def chip_at(d, t):
        return lax.rem(z - t + nz, nz) if d == 0 else lax.rem(z + t, nz)

    def piece(kind, block):
        if kind == KV_N:
            return kv.at[block, pl.ds(0, 2)]
        if kind == KV_W:
            return kv.at[block, pl.ds(2, 3)]
        if kind == UP:
            return up.at[block, pl.ds(pl.multiple_of(hrows * par, hrows), hrows)]
        if kind == DN_A:
            return dn.at[block, pl.ds(qrows, hrows)]
        return dn.at[block, pl.ds(pl.multiple_of(3 * qrows * par, qrows), qrows)]

    def remote(src, dst, send, recv, to):
        return pltpu.make_async_remote_copy(src, dst, send, recv, device_id=to, device_id_type=MESH)

    def z_send(kind, d, t):
        ref = piece(kind, 2 * chip_at(d, t) + c)
        return remote(ref, ref, zs.at[kind, d, t], zr.at[kind, d, t + 1], z_to[d])

    def z_recv(kind, d, t):
        ref = piece(kind, 2 * chip_at(d, t) + c)
        return remote(ref, ref, zs.at[kind, d, 0], zr.at[kind, d, t], z_to[d])

    def core_piece(kind, block):
        if kind == C_KV_N:
            return kv.at[block, pl.ds(0, 2)]
        if kind == C_KV_W:
            return kv.at[block, pl.ds(2, 3)]
        return (up if kind == C_UP else dn).at[block]

    def core_send(kind, d, t):
        ref = core_piece(kind, 2 * chip_at(d, t) + c)
        return remote(ref, ref, cs.at[kind, d, t], cr.at[kind, d, t], core_to)

    def core_recv(kind, d, t, chip):
        ref = core_piece(kind, 2 * chip + 1 - c)
        return remote(ref, ref, cs.at[kind, 0, 0], cr.at[kind, d, t], core_to)

    def y_piece(kind, block, side):
        if kind == Y_UP:
            return up.at[block, pl.ds(pl.multiple_of(hrows * side, hrows), hrows)]
        return dn.at[block, pl.ds(pl.multiple_of(3 * qrows * side, qrows), qrows)]

    def y_send(kind, d, t):
        ref = y_piece(kind, 2 * chip_at(d, t) + c, par)
        return remote(ref, ref, ys.at[kind, d, t], yr.at[kind, d, t], y_to)

    def y_recv(kind, d, t):
        ref = y_piece(kind, 2 * chip_at(d, t) + c, 1 - par)
        return remote(ref, ref, ys.at[kind, d, t], yr.at[kind, d, t], y_to)

    def x_send(d):
        ref = outs.at[j, c]
        return remote(ref, ref, xs.at[d], xr.at[d], {"tp": tp_at(1 - 2 * d)})

    def x_recv(d):
        ref = outs.at[tp_at(2 * d - 1), c]
        return remote(ref, ref, xs.at[d], xr.at[d], {"tp": tp_at(1 - 2 * d)})

    def x_half(owner, d):
        n = outs.shape[2] // 2
        return outs.at[owner, c, pl.ds(n * d, n)]

    def x_relay(d):
        ref = x_half(tp_at(2 * d - 1), d)
        return remote(ref, ref, xs.at[2 + d], xr.at[2 + d], {"tp": tp_at(1 - 2 * d)})

    def x_relayed(d):
        ref = x_half(tp_at(2), d)
        return remote(ref, ref, xs.at[2 + d], xr.at[2 + d], {"tp": tp_at(1 - 2 * d)})

    def o_core(delta, mine):
        ref = outs.at[tp_at(delta), c if mine else 1 - c]
        return remote(ref, ref, os_.at[delta - 1], or_.at[delta - 1], core_to)

    def r_send(delta):
        ref = resid.at[j]
        return remote(ref, ref, rs.at[delta - 1], rr.at[delta - 1], {"tp": tp_at(delta)})

    def r_recv(delta):
        ref = resid.at[tp_at(-delta)]
        return remote(ref, ref, rs.at[delta - 1], rr.at[delta - 1], {"tp": tp_at(delta)})

    def a_send(kind, delta):
        ref = att.at[j, kind]
        return remote(ref, ref, as_.at[kind, delta - 1], ar.at[kind, delta - 1], {"tp": tp_at(delta)})

    def a_recv(kind, delta):
        ref = att.at[tp_at(-delta), kind]
        return remote(ref, ref, as_.at[kind, delta - 1], ar.at[kind, delta - 1], {"tp": tp_at(delta)})

    def m_send(delta, o):
        src = part.at[o, pl.ds(pl.multiple_of(own_rows * tp_at(delta), own_rows), own_rows)]
        dst = mix.at[delta - 1, o]
        return remote(src, dst, ms.at[delta - 1, o], mr.at[delta - 1, o], {"tp": tp_at(delta)})

    def takes(kind, d, t):
        return t <= (half if LAST_WAY[kind] == d else half - 1)

    def passes(kind, d, t):
        return t <= (half - 1 if LAST_WAY[kind] == d else half - 2)

    def when(condition, run):
        if isinstance(condition, bool):
            if condition:
                run()
        else:
            pl.when(condition)(run)

    barrier = pltpu.get_barrier_semaphore()
    friends = [z_to[0], z_to[1], core_to, y_to] + [{"tp": tp_at(k)} for k in range(1, ntp)]
    for friend in friends:
        pl.semaphore_signal(barrier, inc=1, device_id=friend, device_id_type=MESH)
    kd = kv.shape[3]
    local = [
        pltpu.make_async_copy(src, dst, ls.at[i])
        for i, (src, dst) in enumerate(
            [
                (kn_ref, kv.at[s, 0]),
                (vn_ref, kv.at[s, 1]),
                (kw_ref.at[:, pl.ds(0, kd)], kv.at[s, 2]),
                (kw_ref.at[:, pl.ds(kd, kd)], kv.at[s, 3]),
                (vw_ref, kv.at[s, 4]),
                (up_ref, up.at[s]),
                (dn_ref, dn.at[s]),
                (on_ref, outs.at[j, 0]),
                (ow_ref, outs.at[j, 1]),
                (res_ref, resid.at[j]),
            ]
        )
    ]
    for copy in local:
        copy.start()
    acc[...] = jnp.zeros_like(acc)
    top[...] = jnp.full_like(top, -jnp.inf)
    pl.semaphore_wait(barrier, len(friends))
    for copy in local:
        copy.wait()
    for kind in (KV_N, KV_W, UP):
        for d in range(2):
            z_send(kind, d, 0).start()
        core_send((C_KV_N, C_KV_W, C_UP)[kind], 0, 0).start()
    for d in range(2):
        x_send(d).start()
    for delta in range(1, ntp):
        r_send(delta).start()
    core_send(C_DN, 0, 0).start()

    def pump(kind, t):
        for d in range(2):

            def arrived(d=d):
                z_recv(kind, d, t).wait_recv()

                def forward():
                    z_send(kind, d, t).start()

                when(passes(kind, d, t), forward)
                if kind in (KV_N, KV_W):
                    core_send((C_KV_N, C_KV_W)[kind], d, t).start()
                if kind == UP:
                    y_send(Y_UP, d, t).start()
                if kind == DN_B:
                    y_send(Y_DN, d, t).start()

            when(takes(kind, d, t), arrived)

    def complete(y_kind, core_kind, kind, t):
        for d in range(2):

            def done(d=d):
                y_recv(y_kind, d, t).wait_recv()
                core_send(core_kind, d, t).start()

            when(takes(kind, d, t), done)

    ones = jnp.ones((2 * rows, acc.shape[2] - kd), BF16)

    def attend(unit, chip):
        scale = widths[unit] ** -0.5 * LOG2E
        keys = kv[pl.ds(2 * chip, 2), KEY_PART[unit]].reshape(2 * rows, kd)
        values = kv[pl.ds(2 * chip, 2), VALUE_PART[unit]].reshape(2 * rows, kd)
        values = jnp.concatenate([values, ones], axis=1)
        lanes = top.shape[2]
        for row in range(0, q_ref.shape[1], Q_TILE):
            tile = pl.ds(row, Q_TILE)
            scores = lax.dot_general(
                q_ref[unit, tile], keys, (((1,), (1,)), ((), ())), preferred_element_type=F32
            )
            old = top[unit, tile]
            new = jnp.maximum(old, jnp.max(scores, axis=1, keepdims=True))
            rescale = jnp.exp2((old - new) * scale)
            top[unit, tile] = new
            wide = jnp.concatenate([new] * (2 * rows // lanes), axis=1)
            powers = jnp.exp2((scores - wide) * scale).astype(BF16)
            weighted = jnp.dot(powers, values, preferred_element_type=F32)
            wide = jnp.concatenate([rescale] * (acc.shape[2] // lanes), axis=1)
            acc[unit, tile] = acc[unit, tile] * wide + weighted

    def step(t, _):
        dt = t - 1
        chips = jnp.where((dt == 0) | (dt == half), 1, 2)

        def over(units, core_kind):
            def one(i, _):
                chip = lax.rem(jnp.where(i == 0, z - dt, z + dt) + nz, nz)
                if core_kind is not None:
                    way = jnp.where(dt == half, CORE_LAST[core_kind], i)
                    core_recv(core_kind, way, dt, chip).wait_recv()
                for unit in units:
                    attend(unit, chip)
                return 0

            lax.fori_loop(0, chips, one, 0)

        more = t <= half
        over((0, 1), C_KV_N)
        pl.when(more)(lambda: pump(KV_N, t))
        over((2,), C_KV_W)
        pl.when(more)(lambda: pump(KV_W, t))
        over((3,), None)
        pl.when(more)(lambda: pump(UP, t))

        @pl.when(dt >= 1)
        def _():
            complete(Y_UP, C_UP, UP, dt)

        @pl.when(t == half // 2)
        def _():
            for d in range(2):
                x_recv(d).wait_recv()
                x_relay(d).start()

        @pl.when(t == half - 1)
        def _():
            for d in range(2):
                x_relayed(d).wait_recv()
            for delta in range(1, ntp):
                o_core(delta, True).start()

        @pl.when(t == half)
        def _():
            for kind in (DN_A, DN_B):
                for d in range(2):
                    z_send(kind, d, 0).start()

        return 0

    lax.fori_loop(1, half + 2, step, 0)

    def head_group(kind, lam_ref):
        for h in range(2):
            tile = pl.ds(h * rows, rows)
            one = acc[2 * kind, tile]
            two = acc[2 * kind + 1, tile]
            diff = one[:, :kd] / one[:, kd:] - lam_ref[h] * (two[:, :kd] / two[:, kd:])
            square = jnp.mean(diff * diff, axis=-1, keepdims=True)
            diff = diff * lax.rsqrt(square + NORM_EPS) * head_gain_ref[...] * OUT_SCALE
            att[j, kind, :, pl.ds(h * kd, kd)] = diff.astype(BF16)

    head_group(0, lam_n_ref)
    head_group(1, lam_w_ref)
    for kind in range(2):
        for delta in range(1, ntp):
            a_send(kind, delta).start()
    for t in range(1, 4):
        pump(DN_A, t)
        pump(DN_B, t)
        if t > 1:
            complete(Y_DN, C_DN, DN_B, t - 1)
    for delta in range(1, ntp):
        o_core(delta, False).wait_recv()
        r_recv(delta).wait_recv()
        for kind in range(2):
            a_recv(kind, delta).wait_recv()

    sumsq[...] = jnp.zeros_like(sumsq)
    width = mid.shape[1]

    def project(n, _):
        cols = pl.ds(pl.multiple_of(n * COLS, COLS), COLS)
        total = resid[:, :, cols].reshape(mid.shape[0], COLS).astype(F32)
        terms = jnp.zeros((mid.shape[0], COLS), F32)
        for peer in range(ntp):
            term = jnp.dot(att[peer, 0], outs[peer, 0, :, cols], preferred_element_type=F32)
            term = term + jnp.dot(att[peer, 1], outs[peer, 1, :, cols], preferred_element_type=F32)
            terms = terms + term.astype(BF16).astype(F32)
        total = (total + terms).astype(BF16)
        mid[:, cols] = total
        total = total.astype(F32)
        sumsq[...] += jnp.sum(total * total, axis=1, keepdims=True)
        return 0

    lax.fori_loop(0, width // COLS, project, 0)
    pump(DN_A, 4)
    pump(DN_B, 4)
    complete(Y_DN, C_DN, DN_B, 3)

    inverse = lax.rsqrt(sumsq[:, 0:1] * (1.0 / width) + NORM_EPS)

    def normalise(n, _):
        cols = pl.ds(pl.multiple_of(n * COLS, COLS), COLS)
        scaled = mid[:, cols].astype(F32) * inverse
        nrm[:, cols] = (scaled * norm_gain_ref[:, cols].astype(F32)).astype(BF16)
        return 0

    lax.fori_loop(0, width // COLS, normalise, 0)

    def up_wait(t, _):
        for d in range(2):

            def here(d=d):
                core_recv(C_UP, d, t, chip_at(d, t)).wait_recv()

            if d == 0:
                pl.when(t <= half - 1)(here)
            else:
                pl.when(t >= 1)(here)
        return 0

    lax.fori_loop(0, half + 1, up_wait, 0)

    def lift(n, _):
        cols = pl.ds(pl.multiple_of(n * COLS, COLS), COLS)
        weights = up[:, :, cols].reshape(width, COLS)
        lifted = jnp.dot(nrm[...], weights, preferred_element_type=F32)
        lifted = jnp.maximum(lifted, 0.0)
        act[:, cols] = (lifted * lifted).astype(BF16)
        return 0

    lift_steps = act.shape[1] // COLS
    lax.fori_loop(0, lift_steps // 2, lift, 0)
    pump(DN_A, 5)
    pump(DN_B, 5)
    complete(Y_DN, C_DN, DN_B, 4)
    lax.fori_loop(lift_steps // 2, lift_steps, lift, 0)

    def lower(o, t, chip, d):
        core_recv(C_DN, d, t, chip).wait_recv()
        weights = dn[pl.ds(2 * chip, 2)].reshape(2 * wrows, dn.shape[2])
        lowered = lax.dot_general(
            act[...], weights, (((1,), (1,)), ((), ())), preferred_element_type=F32
        )
        part[o] = lowered.astype(BF16)

    def lower_step(t):
        if t == 0:
            lower(0, 0, z, 0)
            done = (0,)
        elif t == half:
            lower(2 * half - 1, half, chip_at(1, half), 1)
            done = (2 * half - 1,)
        else:
            lower(2 * t - 1, t, chip_at(0, t), 0)
            lower(2 * t, t, chip_at(1, t), 1)
            done = (2 * t - 1, 2 * t)
        for o in done:
            for delta in range(1, ntp):
                m_send(delta, o).start()

    for t in range(0, half + 1):
        if t + 6 <= half:
            pump(DN_A, t + 6)
            pump(DN_B, t + 6)
        if t + 5 <= half:
            complete(Y_DN, C_DN, DN_B, t + 5)
        lower_step(t)

    own = pl.ds(pl.multiple_of(own_rows * j, own_rows), own_rows)

    def finish(o, _):
        t = (o + 1) // 2
        chip = lax.rem(jnp.where(o % 2 == 1, z - t, z + t) + nz, nz)
        cols = pl.ds(pl.multiple_of(chip * 2 * wrows, 2 * wrows), 2 * wrows)
        total = part[o, own].astype(F32)
        for delta in range(1, ntp):
            m_send(delta, o).wait_recv()
            total = total + mix[delta - 1, o].astype(F32)
        out_ref[:, cols] = (mid[own, cols].astype(F32) + total).astype(BF16)
        return 0

    lax.fori_loop(0, nz, finish, 0)

    def sent(t, _):
        for kind in range(5):
            for d in range(2):
                pl.when(passes(kind, d, t))(lambda kind=kind, d=d: z_send(kind, d, t).wait_send())
        for kind in range(4):
            for d in range(2):
                last = half if CORE_LAST[kind] == d else half - 1
                first = d
                pl.when((t >= first) & (t <= last))(
                    lambda kind=kind, d=d: core_send(kind, d, t).wait_send()
                )
        for kind in range(2):
            for d in range(2):
                last = half if d == 1 else half - 1
                pl.when((t >= 1) & (t <= last))(
                    lambda kind=kind, d=d: y_send(kind, d, t).wait_send()
                )
        return 0

    lax.fori_loop(0, half + 1, sent, 0)
    for d in range(2):
        x_send(d).wait_send()
        x_relay(d).wait_send()
    for delta in range(1, ntp):
        o_core(delta, True).wait_send()
        r_send(delta).wait_send()
        for kind in range(2):
            a_send(kind, delta).wait_send()

    def mix_sent(o, _):
        for delta in range(1, ntp):
            m_send(delta, o).wait_send()
        return 0

    lax.fori_loop(0, nz, mix_sent, 0)


def shards(
    nsp, ntp,
    resid_in, query_narrow, key_narrow, value_narrow, query_wide, key_wide, value_wide,
    lambda_narrow, lambda_wide, head_gain, out_narrow, out_wide, norm_gain, up_weight, down_weight,
):
    rows, heads, full = query_narrow.shape
    narrow, wide = full // 2, query_wide.shape[2] // 2
    width = resid_in.shape[1]
    hidden = up_weight.shape[1]
    qn = jnp.swapaxes(query_narrow, 0, 1).reshape(heads * rows, full)
    blank = jnp.zeros((heads * rows, narrow), BF16)
    qw = jnp.swapaxes(query_wide, 0, 1).reshape(heads * rows, 2 * wide)
    queries = jnp.stack(
        [
            jnp.concatenate([qn[:, :narrow], blank], axis=1),
            jnp.concatenate([blank, qn[:, narrow:]], axis=1),
            qw[:, :wide],
            qw[:, wide:],
        ]
    )
    nz = nsp // 2
    half = nz // 2
    anywhere = pl.BlockSpec(memory_space=pl.ANY)
    vmem = pl.BlockSpec(memory_space=pltpu.VMEM)
    smem = pl.BlockSpec(memory_space=pltpu.SMEM)
    dma = pltpu.SemaphoreType.DMA
    own_rows = resid_in.shape[0]
    out_rows = out_narrow.shape[0]
    down = down_weight.T
    return pl.pallas_call(
        functools.partial(layer_kernel, nz, ntp, (narrow, narrow, wide, wide)),
        out_shape=jax.ShapeDtypeStruct(resid_in.shape, BF16),
        in_specs=[vmem] + [anywhere] * 9 + [smem, smem, vmem, vmem],
        out_specs=vmem,
        scratch_shapes=[
            pltpu.VMEM((nsp, 5, rows, wide), BF16),
            pltpu.VMEM((nsp, up_weight.shape[0], hidden), BF16),
            pltpu.VMEM((nsp, down.shape[0], hidden), BF16),
            pltpu.VMEM((ntp, 2, out_rows, width), BF16),
            pltpu.VMEM((ntp, own_rows, width), BF16),
            pltpu.VMEM((4, heads * rows, 2 * wide), F32),
            pltpu.VMEM((4, heads * rows, 128), F32),
            pltpu.VMEM((ntp, 2, rows, out_rows), BF16),
            pltpu.VMEM((rows, width), BF16),
            pltpu.VMEM((rows, width), BF16),
            pltpu.VMEM((rows, hidden), BF16),
            pltpu.VMEM((nz, rows, 2 * down.shape[0]), BF16),
            pltpu.VMEM((ntp - 1, nz, own_rows, 2 * down.shape[0]), BF16),
            pltpu.VMEM((rows, 128), F32),
            dma((5, 2, half)),
            dma((5, 2, half + 1)),
            dma((4, 2, half + 1)),
            dma((4, 2, half + 1)),
            dma((2, 2, half + 1)),
            dma((2, 2, half + 1)),
            dma((4,)),
            dma((4,)),
            dma((ntp - 1,)),
            dma((ntp - 1,)),
            dma((ntp - 1,)),
            dma((ntp - 1,)),
            dma((2, ntp - 1)),
            dma((2, ntp - 1)),
            dma((ntp - 1, nz)),
            dma((ntp - 1, nz)),
            dma((10,)),
        ],
        compiler_params=pltpu.CompilerParams(
            collective_id=0, has_side_effects=True, vmem_limit_bytes=62 * 1024 * 1024
        ),
        name="layer",
    )(
        queries,
        key_narrow.reshape(rows, full),
        value_narrow.reshape(rows, -1),
        key_wide.reshape(rows, 2 * wide),
        value_wide.reshape(rows, -1),
        up_weight,
        down,
        out_narrow,
        out_wide,
        resid_in,
        lambda_narrow,
        lambda_wide,
        head_gain.reshape(1, -1),
        norm_gain.reshape(1, -1),
    )


def solution(mesh):
    placed = (
        P(("grp", "sp", "tp"), None),
        P(("grp", "sp"), "tp", None),
        P(("grp", "sp"), "tp", None),
        P(("grp", "sp"), "tp", None),
        P(("grp", "sp"), "tp", None),
        P(("grp", "sp"), "tp", None),
        P(("grp", "sp"), "tp", None),
        P("tp"),
        P("tp"),
        P(),
        P("tp", None),
        P("tp", None),
        P(),
        P("sp", "tp"),
        P("tp", "sp"),
    )
    return jax.shard_map(
        functools.partial(shards, mesh.shape["sp"], mesh.shape["tp"]),
        mesh=mesh,
        in_specs=placed,
        out_specs=P(("grp", "sp", "tp"), None),
        check_vma=False,
    )
```

time: 388 us -> 169 us (0.44)
  Pallas kernels: 0 us -> 162 us
  waiting for transfers between devices: 122 us -> 0 us
  local copies, waits for them, and re-layouts: 109 us -> 4.14 us
  matrix products: 94.4 us -> 0 us
  other arithmetic: 18.6 us -> 0.87 us
  blocking collectives: 16.3 us -> 0 us
  between operations: 13.4 us -> 0.06 us
  starting transfers between devices: 8.37 us -> 0 us
    pallas_call x0 -> x1, Pallas kernels: none -> 162 us  [shards(): pl.pallas_call(functools.partial(layer_kernel, nz, ntp, (narrow, narrow,...]
    dot_general x67 -> x0, matrix products: 94.4 us -> none  [the longest x32 52.6 us: visit(): jnp.einsum('iodph,hie->iodpe', powers.astype(jnp.bfloat16), value_blk, pr...]
    all_gather x3 -> x0, waiting for transfers between devices: 90.5 us -> none  [the longest x1 90.5 us: sent_together(): lax.all_gather(both, axis, axis=dim, tiled=True)]
    while x226 -> x0, local copies, waits for them, and re-layouts: 57.4 us -> none
    all_to_all x2 -> x0, waiting for transfers between devices: 30 us -> none  [the longest x1 15.6 us: sent_and_summed(): parts = lax.all_to_all(split_up(array, dim, peers), axis, 0, 0, tiled=True)]
    dynamic_slice x16 -> x0, local copies, waits for them, and re-layouts: 18.2 us -> none  [absorb(): outcome, _ = lax.scan(visit, states, (key_block_list, value_blocks))]
    all_to_all x1 -> x0, blocking collectives: 16.3 us -> none  [sent_and_summed(): parts = lax.all_to_all(split_up(array, dim, peers), axis, 0, 0, tiled=True)]
    another operation x32 -> x1, other arithmetic: 13 us -> 0.86 us  [shards(): jnp.stack([jnp.concatenate([qn[:, :narrow], blank], axis=1), jnp.concaten...]
  transfers between devices with their start and end apart: 5 -> 0, of which waited for: 3 -> 0; matrix products, arithmetic and copies ran while one was open for 40% -> 0% of each run, Pallas kernels for 0% -> 0%
where the time goes in v1:
time: 169 us; the launch traced here: 167 us
  Pallas kernels  162 us (96%)
  local copies, waits for them, and re-layouts  4.14 us (2%)
    pallas_call x1, Pallas kernels, shards(): pl.pallas_call(functools.partial(layer_kernel, nz, ntp, (narrow, narrow,...  162 us

profile of v1, /device:TPU:40, one launch (start us, length us, event | category | flops | bytes accessed | tf_op | source)
XLA Modules:
  0.0 167.5 jit_solution(15717868445404723154)
XLA Ops:
  0.0 0.0 copy-start
  0.0 1.0 copy.16
  1.0 0.1 slice.14
  1.1 0.0 copy-done
  1.1 0.1 slice_bitcast_fusion.1
  1.2 0.0 copy-start.2
  1.2 0.6 copy-done.2
  1.9 0.0 copy-start.1
  1.9 0.9 pad_maximum_fusion.q_ref
  2.8 0.0 copy-done.1
  2.8 0.6 reshape.56.norm_gain_ref
  3.4 162.4 %layer.1 = bf16[64,2048]{1,0:T(8,128)(2,1)} custom-call(bf16[4,512,128]{2,1,0:T(8,128)(2,1)} %pad_maximum_fusion.q_ref, bf16[256,128]{1,0:T(8,128)(2,1)} %bitcast.26, bf16[256,128]{1,0:T(8,128)(2,1)} %bitcast.27, bf16[256,256]{1,0:T(8,128)(2,1)} %bitcast.24, bf16[256,128]{1,0:T(8,128)(2,1)} %bitcast.28, bf16[64,2048]{1,0:T(8,128)(2,1)} %up_ref.1, ...), custom_call_target="tpu_custom_call" | custom-call | tf_op jit(solution)/shard_map/layer/pallas_call | solution.py:508
  165.8 1.7 copy.20
  (2 shorter events, 0.0 us)
Async XLA Ops:
  0.0 1.1 copy-start
  1.2 0.7 copy-start.2
  1.9 0.9 copy-start.1

commit v2 on v1

v2 whole, which is shorter than its diff:
```python
import functools
import math

import jax
import jax.numpy as jnp
from jax import lax
from jax.experimental import pallas as pl
from jax.experimental.pallas import tpu as pltpu
from jax.sharding import PartitionSpec as P

NORM_EPS = 1e-06
OUT_SCALE = 0.8
LOG2E = math.log2(math.e)
MESH = pl.DeviceIdType.MESH
BF16 = jnp.bfloat16
F32 = jnp.float32

KV_N, KV_W, UP, DN_1, DN_2, DN_Y = range(6)
LAST_WAY = (1, 0, 1, 0, 1, 1)
C_KV_N, C_KV_W, C_DN, C_UP = range(4)
CORE_LAST = (1, 0, 1, 1)
Y_UP, Y_DN = range(2)
KEY_PART = (0, 0, 2, 3)
VALUE_PART = (1, 1, 4, 4)
Q_TILE = 128
COLS = 512
GROUPS = ((0, 1, 2), (3, 4), (5, 6), (7,), (8,))


def layer_kernel(
    nz, ntp, widths,
    qn_ref, qw_ref, kn_ref, vn_ref, kw_ref, vw_ref, up_ref, dn_ref, on_ref, ow_ref, res_ref,
    lam_n_ref, lam_w_ref, head_gain_ref, norm_gain_ref,
    out_ref,
    q, kv, up, dn, outs, resid, acc, top, att, mid, nrm, act, part, mix, sumsq,
    zs, zr, cs, cr, cu, ys, yr, xs, xr, os_, or_, rs, rr, as_, ar, ms, mr, ls,
):
    g, s, j = lax.axis_index("grp"), lax.axis_index("sp"), lax.axis_index("tp")
    z, c = s // 2, s % 2
    par = g % 2
    half = nz // 2
    rows = kv.shape[2]
    wrows = up.shape[1]
    hrows = wrows // 2
    qrows = wrows // 4
    own_rows = resid.shape[1]

    def sp_of(chip):
        return {"sp": 2 * lax.rem(chip + nz, nz) + c}

    z_to = (sp_of(z + 1), sp_of(z - 1))
    core_to = {"sp": 2 * z + 1 - c}
    y_to = {"grp": g + 1 - 2 * par}

    def tp_at(delta):
        return lax.rem(j + delta + ntp, ntp)

    def chip_at(d, t):
        return lax.rem(z - t + nz, nz) if d == 0 else lax.rem(z + t, nz)

    def slot(d, t):
        if isinstance(t, int) and isinstance(d, int):
            return 0 if t == 0 else 2 * half - 1 if t == half else 2 * t - 1 + d
        return jnp.where(t == 0, 0, jnp.where(t == half, 2 * half - 1, 2 * t - 1 + d))

    def piece(kind, block):
        if kind == KV_N:
            return kv.at[block, pl.ds(0, 2)]
        if kind == KV_W:
            return kv.at[block, pl.ds(2, 3)]
        if kind == UP:
            return up.at[block, pl.ds(pl.multiple_of(hrows * par, hrows), hrows)]
        if kind in (DN_1, DN_2):
            return dn.at[block, pl.ds(qrows * (1 + kind - DN_1), qrows)]
        return dn.at[block, pl.ds(pl.multiple_of(3 * qrows * par, qrows), qrows)]

    def remote(src, dst, send, recv, to):
        return pltpu.make_async_remote_copy(src, dst, send, recv, device_id=to, device_id_type=MESH)

    def z_send(kind, d, t):
        ref = piece(kind, 2 * chip_at(d, t) + c)
        return remote(ref, ref, zs.at[kind], zr.at[kind, slot(d, t + 1) - 1], z_to[d])

    def z_recv(kind, d, t):
        ref = piece(kind, 2 * chip_at(d, t) + c)
        return remote(ref, ref, zs.at[kind], zr.at[kind, slot(d, t) - 1], z_to[d])

    def core_piece(kind, block):
        if kind == C_KV_N:
            return kv.at[block, pl.ds(0, 2)]
        if kind == C_KV_W:
            return kv.at[block, pl.ds(2, 3)]
        return (up if kind == C_UP else dn).at[block]

    def core_got(kind, d, t):
        return cu.at[0] if kind == C_UP else cr.at[kind, slot(d, t)]

    def core_send(kind, d, t):
        ref = core_piece(kind, 2 * chip_at(d, t) + c)
        return remote(ref, ref, cs.at[kind], core_got(kind, d, t), core_to)

    def core_recv(kind, d, t, chip):
        ref = core_piece(kind, 2 * chip + 1 - c)
        return remote(ref, ref, cs.at[kind], core_got(kind, d, t), core_to)

    def y_piece(kind, block, side):
        if kind == Y_UP:
            return up.at[block, pl.ds(pl.multiple_of(hrows * side, hrows), hrows)]
        return dn.at[block, pl.ds(pl.multiple_of(3 * qrows * side, qrows), qrows)]

    def y_send(kind, d, t):
        ref = y_piece(kind, 2 * chip_at(d, t) + c, par)
        return remote(ref, ref, ys.at[kind], yr.at[kind, slot(d, t) - 1], y_to)

    def y_recv(kind, d, t):
        ref = y_piece(kind, 2 * chip_at(d, t) + c, 1 - par)
        return remote(ref, ref, ys.at[kind], yr.at[kind, slot(d, t) - 1], y_to)

    def x_send(d):
        ref = outs.at[j, c]
        return remote(ref, ref, xs.at[d], xr.at[d], {"tp": tp_at(1 - 2 * d)})

    def x_recv(d):
        ref = outs.at[tp_at(2 * d - 1), c]
        return remote(ref, ref, xs.at[d], xr.at[d], {"tp": tp_at(1 - 2 * d)})

    def x_half(owner, d):
        n = outs.shape[2] // 2
        return outs.at[owner, c, pl.ds(n * d, n)]

    def x_relay(d):
        ref = x_half(tp_at(2 * d - 1), d)
        return remote(ref, ref, xs.at[2 + d], xr.at[2 + d], {"tp": tp_at(1 - 2 * d)})

    def x_relayed(d):
        ref = x_half(tp_at(2), d)
        return remote(ref, ref, xs.at[2 + d], xr.at[2 + d], {"tp": tp_at(1 - 2 * d)})

    def o_core(delta, mine):
        ref = outs.at[tp_at(delta), c if mine else 1 - c]
        return remote(ref, ref, os_.at[0], or_.at[0], core_to)

    def r_send(delta):
        ref = resid.at[j]
        return remote(ref, ref, rs.at[0], rr.at[0], {"tp": tp_at(delta)})

    def r_recv(delta):
        ref = resid.at[tp_at(-delta)]
        return remote(ref, ref, rs.at[0], rr.at[0], {"tp": tp_at(delta)})

    def a_send(kind, delta):
        ref = att.at[j, kind]
        return remote(ref, ref, as_.at[0], ar.at[0], {"tp": tp_at(delta)})

    def a_recv(kind, delta):
        ref = att.at[tp_at(-delta), kind]
        return remote(ref, ref, as_.at[0], ar.at[0], {"tp": tp_at(delta)})

    def m_send(delta, group):
        first = max(2 * GROUPS[group][0] - 1, 0)
        count = min(2 * GROUPS[group][-1], nz - 1) + 1 - first
        rows_to = pl.ds(pl.multiple_of(own_rows * tp_at(delta), own_rows), own_rows)
        src = part.at[pl.ds(first, count), rows_to]
        dst = mix.at[delta - 1, pl.ds(first, count)]
        return remote(src, dst, ms.at[0], mr.at[delta - 1, group], {"tp": tp_at(delta)})

    def all_of(ref, send, recv):
        return remote(ref, ref, send, recv, core_to)

    def takes(kind, d, t):
        return t <= (half if LAST_WAY[kind] == d else half - 1)

    def passes(kind, d, t):
        return t <= (half - 1 if LAST_WAY[kind] == d else half - 2)

    def when(condition, run):
        if isinstance(condition, bool):
            if condition:
                run()
        else:
            pl.when(condition)(run)

    barrier = pltpu.get_barrier_semaphore()
    friends = [z_to[0], z_to[1], core_to, y_to] + [{"tp": tp_at(k)} for k in range(1, ntp)]
    for friend in friends:
        pl.semaphore_signal(barrier, inc=1, device_id=friend, device_id_type=MESH)
    kd = kv.shape[3]
    local = [
        pltpu.make_async_copy(src, dst, ls.at[i])
        for src, dst, i in [
            (kn_ref, kv.at[s, 0], 0),
            (vn_ref, kv.at[s, 1], 0),
            (kw_ref.at[:, pl.ds(0, kd)], kv.at[s, 2], 0),
            (kw_ref.at[:, pl.ds(kd, kd)], kv.at[s, 3], 0),
            (vw_ref, kv.at[s, 4], 0),
            (up_ref, up.at[s], 1),
            (on_ref, outs.at[j, 0], 2),
            (ow_ref, outs.at[j, 1], 2),
            (res_ref, resid.at[j], 3),
            (dn_ref, dn.at[s], 4),
        ]
    ]
    for copy in local:
        copy.start()

    def local_wait(ref, i):
        pltpu.make_async_copy(ref, ref, ls.at[i]).wait()

    pl.semaphore_wait(barrier, len(friends))
    local_wait(kv.at[s], 0)
    for kind in (KV_N, KV_W):
        for d in range(2):
            z_send(kind, d, 0).start()
        core_send((C_KV_N, C_KV_W)[kind], 0, 0).start()
    local_wait(up.at[s], 1)
    for d in range(2):
        z_send(UP, d, 0).start()
    core_send(C_UP, 0, 0).start()
    local_wait(outs.at[j], 2)
    for d in range(2):
        x_send(d).start()
    local_wait(resid.at[j], 3)
    for delta in range(1, ntp):
        r_send(delta).start()
    local_wait(dn.at[s], 4)
    core_send(C_DN, 0, 0).start()

    acc[...] = jnp.zeros_like(acc)
    top[...] = jnp.full_like(top, -jnp.inf)
    narrow_q = qn_ref[...].astype(F32)
    first_map = lax.broadcasted_iota(jnp.int32, narrow_q.shape, 1) < kd // 2
    q[0] = jnp.where(first_map, narrow_q, 0.0).astype(BF16)
    q[1] = jnp.where(first_map, 0.0, narrow_q).astype(BF16)
    q[2] = qw_ref[:, :kd]
    q[3] = qw_ref[:, kd:]

    def pump(kind, t):
        for d in range(2):

            def arrived(d=d):
                z_recv(kind, d, t).wait_recv()

                def forward():
                    z_send(kind, d, t).start()

                when(passes(kind, d, t), forward)
                if kind in (KV_N, KV_W):
                    core_send((C_KV_N, C_KV_W)[kind], d, t).start()
                if kind == UP:
                    y_send(Y_UP, d, t).start()
                if kind == DN_Y:
                    y_send(Y_DN, d, t).start()

            when(takes(kind, d, t), arrived)

    def complete(y_kind, core_kind, kind, t):
        for d in range(2):

            def done(d=d):
                y_recv(y_kind, d, t).wait_recv()
                core_send(core_kind, d, t).start()

            when(takes(kind, d, t), done)

    ones = jnp.ones((2 * rows, acc.shape[2] - kd), BF16)

    def attend(unit, chip):
        scale = widths[unit] ** -0.5 * LOG2E
        keys = kv[pl.ds(2 * chip, 2), KEY_PART[unit]].reshape(2 * rows, kd)
        values = kv[pl.ds(2 * chip, 2), VALUE_PART[unit]].reshape(2 * rows, kd)
        values = jnp.concatenate([values, ones], axis=1)
        lanes = top.shape[2]
        for row in range(0, q.shape[1], Q_TILE):
            tile = pl.ds(row, Q_TILE)
            scores = lax.dot_general(
                q[unit, tile], keys, (((1,), (1,)), ((), ())), preferred_element_type=F32
            )
            old = top[unit, tile]
            new = jnp.maximum(old, jnp.max(scores, axis=1, keepdims=True))
            rescale = jnp.exp2((old - new) * scale)
            top[unit, tile] = new
            wide = jnp.concatenate([new] * (2 * rows // lanes), axis=1)
            powers = jnp.exp2((scores - wide) * scale).astype(BF16)
            weighted = jnp.dot(powers, values, preferred_element_type=F32)
            wide = jnp.concatenate([rescale] * (acc.shape[2] // lanes), axis=1)
            acc[unit, tile] = acc[unit, tile] * wide + weighted

    def head_group(kind, lam_ref):
        for h in range(2):
            tile = pl.ds(h * rows, rows)
            one = acc[2 * kind, tile]
            two = acc[2 * kind + 1, tile]
            diff = one[:, :kd] / one[:, kd:] - lam_ref[h] * (two[:, :kd] / two[:, kd:])
            square = jnp.mean(diff * diff, axis=-1, keepdims=True)
            diff = diff * lax.rsqrt(square + NORM_EPS) * head_gain_ref[...] * OUT_SCALE
            att[j, kind, :, pl.ds(h * kd, kd)] = diff.astype(BF16)

    def step(t, _):
        dt = t - 1
        chips = jnp.where((dt == 0) | (dt == half), 1, 2)

        def over(units, core_kind):
            def one(i, _):
                chip = lax.rem(jnp.where(i == 0, z - dt, z + dt) + nz, nz)
                if core_kind is not None:
                    way = jnp.where(dt == half, CORE_LAST[core_kind], i)
                    core_recv(core_kind, way, dt, chip).wait_recv()
                for unit in units:
                    attend(unit, chip)
                return 0

            lax.fori_loop(0, chips, one, 0)

        more = t <= half
        over((0, 1), C_KV_N)
        pl.when(more)(lambda: pump(KV_N, t))

        @pl.when(t == half + 1)
        def _():
            pump(DN_1, 1)
            head_group(0, lam_n_ref)
            for delta in range(1, ntp):
                a_send(0, delta).start()

        over((2,), C_KV_W)
        pl.when(more)(lambda: pump(KV_W, t))
        pl.when(t == half + 1)(lambda: pump(DN_2, 1))
        over((3,), None)
        pl.when(more)(lambda: pump(UP, t))
        pl.when(t == half + 1)(lambda: pump(DN_Y, 1))

        @pl.when(t == half - 1)
        def _():
            for kind in (DN_1, DN_2, DN_Y):
                for d in range(2):
                    z_send(kind, d, 0).start()

        @pl.when(dt >= 1)
        def _():
            complete(Y_UP, C_UP, UP, dt)

        @pl.when(t == half // 2)
        def _():
            for d in range(2):
                x_recv(d).wait_recv()
                x_relay(d).start()
            o_core(1, True).start()

        pl.when(t == half // 2 + 1)(lambda: o_core(ntp - 1, True).start())

        @pl.when(t == half - 2)
        def _():
            for d in range(2):
                x_relayed(d).wait_recv()
            o_core(2, True).start()

        return 0

    lax.fori_loop(1, half + 2, step, 0)

    head_group(1, lam_w_ref)
    for delta in range(1, ntp):
        a_send(1, delta).start()

    relays = [(kind, t) for t in range(2, half + 1) for kind in (DN_1, DN_2, DN_Y)]

    def relay(count):
        for _ in range(min(count, len(relays))):
            kind, t = relays.pop(0)
            pump(kind, t)
            if kind == DN_Y:
                complete(Y_DN, C_DN, DN_Y, t - 1)

    relay(6)
    all_of(outs.at[pl.ds(0, ntp - 1), 0], os_.at[0], or_.at[0]).wait_recv()
    all_of(resid.at[pl.ds(0, ntp - 1)], rs.at[0], rr.at[0]).wait_recv()
    all_of(att.at[pl.ds(0, ntp - 1)], as_.at[0], ar.at[0]).wait_recv()

    width = mid.shape[1]
    squares = jnp.zeros((mid.shape[0], 128), F32)
    for n in range(0, width, COLS):
        cols = pl.ds(n, COLS)
        total = resid[:, :, cols].reshape(mid.shape[0], COLS).astype(F32)
        terms = jnp.zeros((mid.shape[0], COLS), F32)
        for peer in range(ntp):
            term = jnp.dot(att[peer, 0], outs[peer, 0, :, cols], preferred_element_type=F32)
            term = term + jnp.dot(att[peer, 1], outs[peer, 1, :, cols], preferred_element_type=F32)
            terms = terms + term.astype(BF16).astype(F32)
        total = (total + terms).astype(BF16)
        mid[:, cols] = total
        total = total.astype(F32)
        total = total * total
        for k in range(0, COLS, 128):
            squares = squares + total[:, k : k + 128]
        sumsq[...] = squares
        relay(1)
        squares = sumsq[...]

    inverse = lax.rsqrt(jnp.sum(squares, axis=1, keepdims=True) * (1.0 / width) + NORM_EPS)
    for k in range(width // 128):
        cols = pl.ds(128 * k, 128)
        gain = norm_gain_ref[k : k + 1, :].astype(F32)
        nrm[:, cols] = (mid[:, cols].astype(F32) * inverse * gain).astype(BF16)
    relay(1)

    all_of(up.at[pl.ds(0, nz)], cs.at[C_UP], cu.at[0]).wait_recv()
    for n in range(0, act.shape[1], COLS):
        cols = pl.ds(n, COLS)
        weights = up[:, :, cols].reshape(width, COLS)
        lifted = jnp.dot(nrm[...], weights, preferred_element_type=F32)
        lifted = jnp.maximum(lifted, 0.0)
        act[:, cols] = (lifted * lifted).astype(BF16)
        relay(1)

    def chips_of(t):
        if t in (0, half):
            return [(0 if t == 0 else 1, chip_at(1, t))]
        return [(d, chip_at(d, t)) for d in range(2)]

    def lower(t):
        weights = []
        for d, chip in chips_of(t):
            core_recv(C_DN, d, t, chip).wait_recv()
            weights.append(dn[pl.ds(2 * chip, 2)].reshape(2 * wrows, dn.shape[2]))
        weights = weights[0] if len(weights) == 1 else jnp.concatenate(weights, axis=0)
        lowered = lax.dot_general(
            act[...], weights, (((1,), (1,)), ((), ())), preferred_element_type=F32
        ).astype(BF16)
        for i in range(len(chips_of(t))):
            part[max(2 * t - 1, 0) + i] = lowered[:, 2 * wrows * i : 2 * wrows * (i + 1)]

    own = pl.ds(pl.multiple_of(own_rows * j, own_rows), own_rows)

    def finish(group):
        for delta in range(1, ntp):
            m_send(delta, group).wait_recv()
        for t in GROUPS[group]:
            for i, (_, chip) in enumerate(chips_of(t)):
                o = max(2 * t - 1, 0) + i
                cols = pl.ds(pl.multiple_of(chip * 2 * wrows, 2 * wrows), 2 * wrows)
                total = part[o, own].astype(F32)
                for delta in range(1, ntp):
                    total = total + mix[delta - 1, o].astype(F32)
                out_ref[:, cols] = (mid[own, cols].astype(F32) + total).astype(BF16)

    for group, distances in enumerate(GROUPS):
        for t in distances:
            lower(t)
            relay(1 if t < 4 else 2)
            if t == 5:
                complete(Y_DN, C_DN, DN_Y, half)
        for delta in range(1, ntp):
            m_send(delta, group).start()
        if group > 0:
            finish(group - 1)
    finish(len(GROUPS) - 1)

    blocks = nz - 1
    for kind in (KV_N, KV_W):
        parts = pl.ds(0, 2 if kind == KV_N else 3)
        all_of(kv.at[pl.ds(0, blocks), parts], zs.at[kind], cu.at[0]).wait_send()
        all_of(kv.at[pl.ds(0, nz), parts], cs.at[kind], cu.at[0]).wait_send()
    all_of(up.at[pl.ds(0, blocks), pl.ds(0, hrows)], zs.at[UP], cu.at[0]).wait_send()
    all_of(up.at[pl.ds(0, blocks), pl.ds(0, hrows)], ys.at[Y_UP], cu.at[0]).wait_send()
    for kind in (DN_1, DN_2, DN_Y):
        all_of(dn.at[pl.ds(0, blocks), pl.ds(0, qrows)], zs.at[kind], cu.at[0]).wait_send()
    all_of(dn.at[pl.ds(0, blocks), pl.ds(0, qrows)], ys.at[Y_DN], cu.at[0]).wait_send()
    all_of(up.at[pl.ds(0, nz)], cs.at[C_UP], cu.at[0]).wait_send()
    all_of(dn.at[pl.ds(0, nz)], cs.at[C_DN], cu.at[0]).wait_send()
    for d in range(2):
        x_send(d).wait_send()
        x_relay(d).wait_send()
    all_of(outs.at[pl.ds(0, ntp - 1), 0], os_.at[0], or_.at[0]).wait_send()
    all_of(resid.at[pl.ds(0, ntp - 1)], rs.at[0], rr.at[0]).wait_send()
    all_of(att.at[pl.ds(0, ntp - 1)], as_.at[0], ar.at[0]).wait_send()
    all_of(mix, ms.at[0], mr.at[0, 0]).wait_send()


def shards(
    nsp, ntp,
    resid_in, query_narrow, key_narrow, value_narrow, query_wide, key_wide, value_wide,
    lambda_narrow, lambda_wide, head_gain, out_narrow, out_wide, norm_gain, up_weight, down_weight,
):
    rows, heads, full = query_narrow.shape
    narrow, wide = full // 2, query_wide.shape[2] // 2
    width = resid_in.shape[1]
    hidden = up_weight.shape[1]
    qn = jnp.swapaxes(query_narrow, 0, 1).reshape(heads * rows, full)
    qw = jnp.swapaxes(query_wide, 0, 1).reshape(heads * rows, 2 * wide)
    nz = nsp // 2
    anywhere = pl.BlockSpec(memory_space=pl.ANY)
    vmem = pl.BlockSpec(memory_space=pltpu.VMEM)
    smem = pl.BlockSpec(memory_space=pltpu.SMEM)
    dma = pltpu.SemaphoreType.DMA
    own_rows = resid_in.shape[0]
    out_rows = out_narrow.shape[0]
    down = down_weight.T
    return pl.pallas_call(
        functools.partial(layer_kernel, nz, ntp, (narrow, narrow, wide, wide)),
        out_shape=jax.ShapeDtypeStruct(resid_in.shape, BF16),
        in_specs=[vmem, vmem] + [anywhere] * 9 + [smem, smem, vmem, vmem],
        out_specs=vmem,
        scratch_shapes=[
            pltpu.VMEM((4, heads * rows, wide), BF16),
            pltpu.VMEM((nsp, 5, rows, wide), BF16),
            pltpu.VMEM((nsp, up_weight.shape[0], hidden), BF16),
            pltpu.VMEM((nsp, down.shape[0], hidden), BF16),
            pltpu.VMEM((ntp, 2, out_rows, width), BF16),
            pltpu.VMEM((ntp, own_rows, width), BF16),
            pltpu.VMEM((4, heads * rows, 2 * wide), F32),
            pltpu.VMEM((4, heads * rows, 128), F32),
            pltpu.VMEM((ntp, 2, rows, out_rows), BF16),
            pltpu.VMEM((rows, width), BF16),
            pltpu.VMEM((rows, width), BF16),
            pltpu.VMEM((rows, hidden), BF16),
            pltpu.VMEM((nz, rows, 2 * down.shape[0]), BF16),
            pltpu.VMEM((ntp - 1, nz, own_rows, 2 * down.shape[0]), BF16),
            pltpu.VMEM((rows, 128), F32),
            dma((6,)),
            dma((6, nz - 1)),
            dma((4,)),
            dma((3, nz)),
            dma((1,)),
            dma((2,)),
            dma((2, nz - 1)),
            dma((4,)),
            dma((4,)),
            dma((1,)),
            dma((1,)),
            dma((1,)),
            dma((1,)),
            dma((1,)),
            dma((1,)),
            dma((1,)),
            dma((ntp - 1, len(GROUPS))),
            dma((5,)),
        ],
        compiler_params=pltpu.CompilerParams(
            collective_id=0, has_side_effects=True, vmem_limit_bytes=62 * 1024 * 1024
        ),
        name="layer",
    )(
        qn,
        qw,
        key_narrow.reshape(rows, full),
        value_narrow.reshape(rows, -1),
        key_wide.reshape(rows, 2 * wide),
        value_wide.reshape(rows, -1),
        up_weight,
        down,
        out_narrow,
        out_wide,
        resid_in,
        lambda_narrow,
        lambda_wide,
        head_gain.reshape(1, -1),
        norm_gain.reshape(-1, 128),
    )


def solution(mesh):
    placed = (
        P(("grp", "sp", "tp"), None),
        P(("grp", "sp"), "tp", None),
        P(("grp", "sp"), "tp", None),
        P(("grp", "sp"), "tp", None),
        P(("grp", "sp"), "tp", None),
        P(("grp", "sp"), "tp", None),
        P(("grp", "sp"), "tp", None),
        P("tp"),
        P("tp"),
        P(),
        P("tp", None),
        P("tp", None),
        P(),
        P("sp", "tp"),
        P("tp", "sp"),
    )
    return jax.shard_map(
        functools.partial(shards, mesh.shape["sp"], mesh.shape["tp"]),
        mesh=mesh,
        in_specs=placed,
        out_specs=P(("grp", "sp", "tp"), None),
        check_vma=False,
    )
```

time: 169 us -> 157 us (0.929)
  Pallas kernels: 162 us -> 151 us
    pallas_call x1, Pallas kernels: 162 us -> 151 us  [shards(): pl.pallas_call(functools.partial(layer_kernel, nz, ntp, (narrow, narrow,...]
where the time goes in v2:
time: 157 us; the launch traced here: 155 us
  Pallas kernels  151 us (96%)
  local copies, waits for them, and re-layouts  4.03 us (3%)
    pallas_call x1, Pallas kernels, shards(): pl.pallas_call(functools.partial(layer_kernel, nz, ntp, (narrow, narrow,...  151 us

profile of v2, /device:TPU:40, one launch (start us, length us, event | category | flops | bytes accessed | tf_op | source)
XLA Modules:
  0.0 155.5 jit_solution(16396766772036574173)
XLA Ops:
  0.0 0.0 copy-start
  0.0 1.6 %copy.16 = bf16[2,256,128]{2,1,0:T(8,128)(2,1)} copy(bf16[2,256,128]{2,0,1:T(2,128)(2,1)} %bitcast.16) | data formatting | bytes 262144 | tf_op jit(solution)/shard_map/transpose | solution.py:488
  1.6 0.0 copy-done
  1.6 0.7 copy.17
  2.4 151.4 %layer.1 = bf16[64,2048]{1,0:T(8,128)(2,1)} custom-call(bf16[512,128]{1,0:T(8,128)(2,1)} %bitcast.12, bf16[512,256]{1,0:T(8,128)(2,1)} %bitcast.11, bf16[256,128]{1,0:T(8,128)(2,1)} %bitcast.17, bf16[256,128]{1,0:T(8,128)(2,1)} %bitcast.18, bf16[256,256]{1,0:T(8,128)(2,1)} %bitcast.15, bf16[256,128]{1,0:T(8,128)(2,1)} %bitcast.19, bf16[64,2048]{1,0:T(8,128)(2,1)} %up_ref.1, ...), custom_call_target="tpu_custom_call" | custom-call | tf_op jit(solution)/shard_map/layer/pallas_call | solution.py:498
  153.8 1.7 %copy.19 = bf16[64,2048]{1,0:T(8,128)(2,1)} copy(bf16[64,2048]{1,0:T(8,128)(2,1)} %layer.1) | data formatting | bytes 524288
Async XLA Ops:
  0.0 1.6 %copy-start = (bf16[256,2,256]{2,1,0:T(2,128)(2,1)S(1)}, bf16[256,2,256]{2,1,0:T(2,128)(2,1)}, u32[]{:S(2)}) copy-start(bf16[256,2,256]{2,1,0:T(2,128)(2,1)} %param.19) | copy-start | bytes 786436

commit v3 on v2

--- a/solution.py
+++ b/solution.py
@@ -15,8 +15,8 @@
 BF16 = jnp.bfloat16
 F32 = jnp.float32
 
-KV_N, KV_W, UP, DN_1, DN_2, DN_Y = range(6)
-LAST_WAY = (1, 0, 1, 0, 1, 1)
+KV_N, KV_W, UP, DN_Y, DN_1, DN_2 = range(6)
+LAST_WAY = (1, 0, 1, 1, 0, 1)
 C_KV_N, C_KV_W, C_DN, C_UP = range(4)
 CORE_LAST = (1, 0, 1, 1)
 Y_UP, Y_DN = range(2)
@@ -32,7 +32,7 @@
     qn_ref, qw_ref, kn_ref, vn_ref, kw_ref, vw_ref, up_ref, dn_ref, on_ref, ow_ref, res_ref,
     lam_n_ref, lam_w_ref, head_gain_ref, norm_gain_ref,
     out_ref,
-    q, kv, up, dn, outs, resid, acc, top, att, mid, nrm, act, part, mix, sumsq,
+    qn, qw, q, kv, up, dn, outs, resid, acc, top, att, mid, nrm, act, part, mix, sumsq,
     zs, zr, cs, cr, cu, ys, yr, xs, xr, os_, or_, rs, rr, as_, ar, ms, mr, ls,
 ):
     g, s, j = lax.axis_index("grp"), lax.axis_index("sp"), lax.axis_index("tp")
@@ -198,6 +198,8 @@
             (ow_ref, outs.at[j, 1], 2),
             (res_ref, resid.at[j], 3),
             (dn_ref, dn.at[s], 4),
+            (qn_ref, qn, 5),
+            (qw_ref, qw, 6),
         ]
     ]
     for copy in local:
@@ -227,12 +229,19 @@
 
     acc[...] = jnp.zeros_like(acc)
     top[...] = jnp.full_like(top, -jnp.inf)
-    narrow_q = qn_ref[...].astype(F32)
-    first_map = lax.broadcasted_iota(jnp.int32, narrow_q.shape, 1) < kd // 2
-    q[0] = jnp.where(first_map, narrow_q, 0.0).astype(BF16)
-    q[1] = jnp.where(first_map, 0.0, narrow_q).astype(BF16)
-    q[2] = qw_ref[:, :kd]
-    q[3] = qw_ref[:, kd:]
+    local_wait(qn, 5)
+    local_wait(qw, 6)
+    narrow_q = qn[...].astype(F32)
+    wide_q = qw[...].astype(F32)
+    first_map = lax.broadcasted_iota(jnp.int32, (rows, kd), 1) < kd // 2
+    for h in range(2):
+        tile = pl.ds(h * rows, rows)
+        head = narrow_q[:, h, :]
+        q[0, tile] = jnp.where(first_map, head, 0.0).astype(BF16)
+        q[1, tile] = jnp.where(first_map, 0.0, head).astype(BF16)
+        head = wide_q[:, h, :].astype(BF16)
+        q[2, tile] = head[:, :kd]
+        q[3, tile] = head[:, kd:]
 
     def pump(kind, t):
         for d in range(2):
@@ -317,21 +326,21 @@
 
         @pl.when(t == half + 1)
         def _():
-            pump(DN_1, 1)
+            pump(DN_Y, 1)
             head_group(0, lam_n_ref)
             for delta in range(1, ntp):
                 a_send(0, delta).start()
 
         over((2,), C_KV_W)
         pl.when(more)(lambda: pump(KV_W, t))
-        pl.when(t == half + 1)(lambda: pump(DN_2, 1))
+        pl.when(t == half + 1)(lambda: pump(DN_1, 1))
         over((3,), None)
         pl.when(more)(lambda: pump(UP, t))
-        pl.when(t == half + 1)(lambda: pump(DN_Y, 1))
+        pl.when(t == half + 1)(lambda: pump(DN_2, 1))
 
         @pl.when(t == half - 1)
         def _():
-            for kind in (DN_1, DN_2, DN_Y):
+            for kind in (DN_Y, DN_1, DN_2):
                 for d in range(2):
                     z_send(kind, d, 0).start()
 
@@ -362,13 +371,13 @@
     for delta in range(1, ntp):
         a_send(1, delta).start()
 
-    relays = [(kind, t) for t in range(2, half + 1) for kind in (DN_1, DN_2, DN_Y)]
+    relays = [(kind, t) for t in range(2, half + 1) for kind in (DN_Y, DN_1, DN_2)]
 
     def relay(count):
         for _ in range(min(count, len(relays))):
             kind, t = relays.pop(0)
             pump(kind, t)
-            if kind == DN_Y:
+            if kind == DN_1:
                 complete(Y_DN, C_DN, DN_Y, t - 1)
 
     relay(6)
@@ -462,7 +471,7 @@
         all_of(kv.at[pl.ds(0, nz), parts], cs.at[kind], cu.at[0]).wait_send()
     all_of(up.at[pl.ds(0, blocks), pl.ds(0, hrows)], zs.at[UP], cu.at[0]).wait_send()
     all_of(up.at[pl.ds(0, blocks), pl.ds(0, hrows)], ys.at[Y_UP], cu.at[0]).wait_send()
-    for kind in (DN_1, DN_2, DN_Y):
+    for kind in (DN_Y, DN_1, DN_2):
         all_of(dn.at[pl.ds(0, blocks), pl.ds(0, qrows)], zs.at[kind], cu.at[0]).wait_send()
     all_of(dn.at[pl.ds(0, blocks), pl.ds(0, qrows)], ys.at[Y_DN], cu.at[0]).wait_send()
     all_of(up.at[pl.ds(0, nz)], cs.at[C_UP], cu.at[0]).wait_send()
@@ -485,8 +494,6 @@
     narrow, wide = full // 2, query_wide.shape[2] // 2
     width = resid_in.shape[1]
     hidden = up_weight.shape[1]
-    qn = jnp.swapaxes(query_narrow, 0, 1).reshape(heads * rows, full)
-    qw = jnp.swapaxes(query_wide, 0, 1).reshape(heads * rows, 2 * wide)
     nz = nsp // 2
     anywhere = pl.BlockSpec(memory_space=pl.ANY)
     vmem = pl.BlockSpec(memory_space=pltpu.VMEM)
@@ -498,9 +505,11 @@
     return pl.pallas_call(
         functools.partial(layer_kernel, nz, ntp, (narrow, narrow, wide, wide)),
         out_shape=jax.ShapeDtypeStruct(resid_in.shape, BF16),
-        in_specs=[vmem, vmem] + [anywhere] * 9 + [smem, smem, vmem, vmem],
+        in_specs=[anywhere] * 11 + [smem, smem, vmem, vmem],
         out_specs=vmem,
         scratch_shapes=[
+            pltpu.VMEM(query_narrow.shape, BF16),
+            pltpu.VMEM(query_wide.shape, BF16),
             pltpu.VMEM((4, heads * rows, wide), BF16),
             pltpu.VMEM((nsp, 5, rows, wide), BF16),
             pltpu.VMEM((nsp, up_weight.shape[0], hidden), BF16),
@@ -533,15 +542,15 @@
             dma((1,)),
             dma((1,)),
             dma((ntp - 1, len(GROUPS))),
-            dma((5,)),
+            dma((7,)),
         ],
         compiler_params=pltpu.CompilerParams(
             collective_id=0, has_side_effects=True, vmem_limit_bytes=62 * 1024 * 1024
         ),
         name="layer",
     )(
-        qn,
-        qw,
+        query_narrow,
+        query_wide,
         key_narrow.reshape(rows, full),
         value_narrow.reshape(rows, -1),
         key_wide.reshape(rows, 2 * wide),

time: 157 us -> 153 us (0.975); the launches traced: 155 us -> 153 us
  local copies, waits for them, and re-layouts: 4.03 us -> 1.67 us
    transpose x2 -> x0, local copies, waits for them, and re-layouts: 2.35 us -> none  [the longest x1 1.62 us: shards(): qn = jnp.swapaxes(query_narrow, 0, 1).reshape(heads * rows, full)]
where the time goes in v3:
time: 153 us
  Pallas kernels  151 us (99%)
  local copies, waits for them, and re-layouts  1.67 us (1%)
    pallas_call x1, Pallas kernels, shards(): pl.pallas_call(functools.partial(layer_kernel, nz, ntp, (narrow, narrow,...  151 us

profile of v3, /device:TPU:40, one launch (start us, length us, event | category | flops | bytes accessed | tf_op | source)
XLA Modules:
  0.0 153.1 jit_solution(2439733715552282332)
XLA Ops:
  0.0 151.4 %layer.1 = bf16[64,2048]{1,0:T(8,128)(2,1)} custom-call(bf16[256,2,128]{2,1,0:T(2,128)(2,1)} %qn_ref.1, bf16[256,2,256]{2,1,0:T(2,128)(2,1)} %qw_ref.1, bf16[256,128]{1,0:T(8,128)(2,1)} %bitcast.9, bf16[256,128]{1,0:T(8,128)(2,1)} %bitcast.10, bf16[256,256]{1,0:T(8,128)(2,1)} %bitcast.8, bf16[256,128]{1,0:T(8,128)(2,1)} %bitcast.11, ...), custom_call_target="tpu_custom_call" | custom-call | tf_op jit(solution)/shard_map/layer/pallas_call | solution.py:505
  151.4 1.7 %copy.17 = bf16[64,2048]{1,0:T(8,128)(2,1)} copy(bf16[64,2048]{1,0:T(8,128)(2,1)} %layer.1) | data formatting | bytes 524288

commit v4 on v3

--- a/solution.py
+++ b/solution.py
@@ -16,7 +16,7 @@
 F32 = jnp.float32
 
 KV_N, KV_W, UP, DN_Y, DN_1, DN_2 = range(6)
-LAST_WAY = (1, 0, 1, 1, 0, 1)
+LAST_WAY = (1, 0, 1, 1, 0, 0)
 C_KV_N, C_KV_W, C_DN, C_UP = range(4)
 CORE_LAST = (1, 0, 1, 1)
 Y_UP, Y_DN = range(2)
@@ -98,6 +98,9 @@
     def core_send(kind, d, t):
         ref = core_piece(kind, 2 * chip_at(d, t) + c)
         return remote(ref, ref, cs.at[kind], core_got(kind, d, t), core_to)
+
+    def core_part(ref, d, t):
+        return remote(ref, ref, cs.at[C_DN], core_got(C_DN, d, t), core_to)
 
     def core_recv(kind, d, t, chip):
         ref = core_piece(kind, 2 * chip + 1 - c)
@@ -259,6 +262,8 @@
                     y_send(Y_UP, d, t).start()
                 if kind == DN_Y:
                     y_send(Y_DN, d, t).start()
+                if kind in (DN_Y, DN_1, DN_2):
+                    core_part(piece(kind, 2 * chip_at(d, t) + c), d, t).start()
 
             when(takes(kind, d, t), arrived)
 
@@ -267,7 +272,10 @@
 
             def done(d=d):
                 y_recv(y_kind, d, t).wait_recv()
-                core_send(core_kind, d, t).start()
+                if core_kind == C_DN:
+                    core_part(y_piece(Y_DN, 2 * chip_at(d, t) + c, 1 - par), d, t).start()
+                else:
+                    core_send(core_kind, d, t).start()
 
             when(takes(kind, d, t), done)
 

time: 153 us -> 154 us (level)
  Pallas kernels: 151 us -> 153 us
where the time goes in v4:
time: 154 us
  Pallas kernels  153 us (99%)
  local copies, waits for them, and re-layouts  1.67 us (1%)
    pallas_call x1, Pallas kernels, shards(): pl.pallas_call(functools.partial(layer_kernel, nz, ntp, (narrow, narrow,...  153 us

profile of v4, /device:TPU:40, one launch (start us, length us, event | category | flops | bytes accessed | tf_op | source)
XLA Modules:
  0.0 154.2 jit_solution(7650401250443466604)
XLA Ops:
  0.0 152.5 %layer.1 = bf16[64,2048]{1,0:T(8,128)(2,1)} custom-call(bf16[256,2,128]{2,1,0:T(2,128)(2,1)} %qn_ref.1, bf16[256,2,256]{2,1,0:T(2,128)(2,1)} %qw_ref.1, bf16[256,128]{1,0:T(8,128)(2,1)} %bitcast.9, bf16[256,128]{1,0:T(8,128)(2,1)} %bitcast.10, bf16[256,256]{1,0:T(8,128)(2,1)} %bitcast.8, bf16[256,128]{1,0:T(8,128)(2,1)} %bitcast.11, ...), custom_call_target="tpu_custom_call" | custom-call | tf_op jit(solution)/shard_map/layer/pallas_call | solution.py:513
  152.5 1.7 %copy.17 = bf16[64,2048]{1,0:T(8,128)(2,1)} copy(bf16[64,2048]{1,0:T(8,128)(2,1)} %layer.1) | data formatting | bytes 524288
